TPU v7x, 128 devices: a whole 4x4x4 slice. The times are simulated.
128 devices in a mesh: fs: 16 (over z, y), tp: 8 (over x, core).
Axes of the slice: x: 4, y: 4, z: 4, core: 2. Of those that a mesh axis runs over, the one named last changes fastest.
Arguments:
- weights_in: float32 [2, 2048, 5632], P(None, 'fs', 'tp'), may hold values from -6 to 6
- weights_mix: float32 [2048, 2048], P('fs', 'tp'), may hold values from -6 to 6
- momentum_in: float32 [2, 2048, 5632], P(None, 'fs', 'tp'), may hold values from -5 to 5
- momentum_mix: float32 [2048, 2048], P('fs', 'tp'), may hold values from -5 to 5
- grads_in: float32 [2, 2048, 5632], P(None, 'fs', 'tp'), may hold values from -5 to 5
- grads_mix: float32 [2048, 2048], P('fs', 'tp'), may hold values from -5 to 5
Outputs:
- momentum_in_next: float32 [2, 2048, 5632], P(None, 'fs', 'tp')
- momentum_mix_next: float32 [2048, 2048], P('fs', 'tp')
- weights_in_next: float32 [2, 2048, 5632], P(None, 'fs', 'tp')
- weights_mix_next: float32 [2048, 2048], P('fs', 'tp')
- update_in: float32 [2, 2048, 5632], P(None, 'fs', 'tp')
- update_mix: float32 [2048, 2048], P('fs', 'tp')
All inputs are finite; a program needn't handle non-finite values.
Results may differ from a plain program's by a relative error of at most 0.0003.
Values sent between devices are 32-bit elements; how exact they have to be, the bound alone decides.
No kernel may reach another device: no remote copies, remote signals or barrier semaphores. Data moves between devices by JAX's collectives and lax.ppermute only.
A program may use at most 128 MiB of HBM per device.

v0:
```python
import math
import jax
import jax.numpy as jnp
from jax import lax
from jax.sharding import PartitionSpec as P

D = 2048
FF = 5632
ITERS = 3
A_COEF = 3.4445
B_COEF = -4.775
C_COEF = 2.0315
MOMENTUM_DECAY = 0.95
STEP_RATE = 0.02
HIGH = lax.Precision.HIGHEST


def gather_turned(arrays, axis, dims):
    turned = [jnp.moveaxis(a, dim, 0) for a, dim in zip(arrays, dims)]
    both = jnp.concatenate([t.reshape(len(t), -1) for t in turned], axis=1)
    result, at, gathered = (lax.all_gather(both, axis, axis=0, tiled=True), 0, [])
    for t, dim in zip(turned, dims):
        share = result[:, at : at + t[0].size].reshape(-1, *t.shape[1:])
        gathered.append(jnp.moveaxis(share, 0, dim))
        at += t[0].size
    return tuple(gathered)


def rows_for(lines, peers):
    spare = -lines.shape[0] % peers
    if not spare:
        return lines
    return jnp.concatenate([lines, jnp.zeros((spare, *lines.shape[1:]), lines.dtype)])


def sum_by_parts(shard, axis):
    lines = shard.reshape(-1, *shard.shape[1:][-1:])
    own = lax.psum_scatter(
        rows_for(lines, lax.axis_size(axis)), axis, scatter_dimension=0, tiled=True
    )
    whole = lax.all_gather(own, axis).reshape(-1, *lines.shape[1:])
    return lax.slice_in_dim(whole, 0, len(lines)).reshape(shard.shape)


def scale_from(summed):
    return (0.5 * lax.rsqrt(jnp.maximum(summed / D, 1.0)))[:, None, None]


def block_trace(shard, row_start, col_start):
    row_ids = row_start + lax.iota(jnp.int32, shard.shape[1])[:, None]
    col_ids = col_start + lax.iota(jnp.int32, shard.shape[2])[None, :]
    return jnp.sum(jnp.where((row_ids == col_ids)[None], shard, 0.0), axis=(1, 2))


def local(weights_in, weights_mix, momentum_in, momentum_mix, grads_in, grads_mix):
    fs_pos = lax.axis_index("fs")
    tp_pos = lax.axis_index("tp")
    moment_in = MOMENTUM_DECAY * momentum_in + grads_in
    moment_mix = MOMENTUM_DECAY * momentum_mix + grads_mix
    local_in = moment_in
    local_mix = moment_mix[None]
    row_count = local_in.shape[1]
    block_width = local_mix.shape[2]
    for iteration in range(ITERS):
        cols_in, cols_mix = gather_turned((local_in, local_mix), "fs", (1, 1))
        partial_value = jnp.concatenate(
            [
                jnp.einsum("krc,ksc->krs", local_in, cols_in, precision=HIGH),
                jnp.einsum("krc,ksc->krs", local_mix, cols_mix, precision=HIGH),
            ]
        )
        gram_rows = sum_by_parts(partial_value, "tp")
        gram_block = lax.dynamic_slice_in_dim(gram_rows, tp_pos * block_width, block_width, 2)
        if iteration == 0:
            traces = block_trace(gram_block, fs_pos * row_count, tp_pos * block_width)
            scaling = scale_from(lax.psum(traces, ("fs", "tp")))
        factor = scaling if iteration == 0 else jnp.ones_like(scaling)
        gram_cols = lax.all_gather(gram_block, "fs", axis=1, tiled=True)
        square = jnp.einsum("krs,ksc->krc", gram_rows, gram_cols, precision=HIGH)
        poly_mat = factor**2 * B_COEF * gram_block + factor**4 * C_COEF * square
        poly_rows = lax.all_gather(poly_mat, "tp", axis=2, tiled=True)
        local_in = factor[:2] * (
            A_COEF * local_in + jnp.einsum("krs,ksc->krc", poly_rows[:2], cols_in, precision=HIGH)
        )
        local_mix = factor[2:] * (
            A_COEF * local_mix + jnp.einsum("krs,ksc->krc", poly_rows[2:], cols_mix, precision=HIGH)
        )
    step_in = local_in * math.sqrt(max(D, FF))
    step_mix = local_mix[0] * math.sqrt(D)
    return (
        moment_in,
        moment_mix,
        weights_in - STEP_RATE * step_in,
        weights_mix - STEP_RATE * step_mix,
        step_in,
        step_mix,
    )


def solution(mesh):
    in_specs = (
        P(None, "fs", "tp"),
        P("fs", "tp"),
        P(None, "fs", "tp"),
        P("fs", "tp"),
        P(None, "fs", "tp"),
        P("fs", "tp"),
    )
    out_specs = (
        P(None, "fs", "tp"),
        P("fs", "tp"),
        P(None, "fs", "tp"),
        P("fs", "tp"),
        P(None, "fs", "tp"),
        P("fs", "tp"),
    )
    return jax.shard_map(local, mesh=mesh, in_specs=in_specs, out_specs=out_specs, check_vma=False)
```

profile of v0, /device:TPU:1, one launch (start us, length us, event | category | flops | bytes accessed | tf_op | source)
XLA Modules:
  0.0 954.7 jit_solution(4597433947635089846)
XLA Ops:
  10.9 105.9 %all-gather.16.cloned.1.call-done = f32[2048,1664]{0,1:T(8,128)} async-done(((f32[128,1664]{0,1:T(8,128)}), f32[2048,1664]{0,1:T(8,128)}) %all-gather.16.cloned.1.call-update) | async-done | bytes 13631504 | tf_op jit(solution)/shard_map/all_gather | solution.py:21
  116.8 10.4 %slice.58 = f32[2048,1408]{0,1:T(8,128)} slice(f32[2048,1664]{0,1:T(8,128)} %all-gather.16.cloned.1.call-done), slice={[0:2048], [0:1408]} | slice | bytes 23068672 | tf_op jit(solution)/shard_map/slice | solution.py:23
  127.2 9.2 fusion.25
  141.2 33.7 %reduce-scatter.4.cloned.1.call-done = f32[48,2048]{1,0:T(8,128)} async-done(((f32[384,2048]{1,0:T(8,128)}), f32[48,2048]{1,0:T(8,128)}) %reduce-scatter.4.cloned.1.call-update) | async-done | bytes 393232 | tf_op jit(solution)/shard_map/reduce_scatter | solution.py:38
  175.1 31.3 %all-gather.34.cloned.1.call-done = f32[384,2048]{1,0:T(8,128)} async-done(((f32[48,2048]{1,0:T(8,128)}), f32[384,2048]{1,0:T(8,128)}) %all-gather.34.cloned.1.call-update) | async-done | bytes 3145744 | tf_op jit(solution)/shard_map/all_gather | solution.py:41
  208.3 67.5 %psum.7 = f32[3]{0:T(128)S(1)} all-reduce(f32[3]{0:T(128)S(1)} %get-tuple-element.8), channel_id=1, replica_groups=mesh['fs'=16,'tp'=8] {'fs','tp'}, use_global_device_ids=true, to_apply=%region_2.3 | all-reduce | flops 3 | bytes 24 | tf_op jit(solution)/shard_map/psum | solution.py:76
  284.9 23.8 %all-gather.20.cloned.1.call-done = f32[3,128,2048]{2,1,0:T(8,128)} async-done(((f32[3,128,256]{2,1,0:T(8,128)}), f32[3,128,2048]{2,1,0:T(8,128)}) %all-gather.20.cloned.1.call-update) | async-done | bytes 3145744 | tf_op jit(solution)/shard_map/all_gather | solution.py:81
  313.6 13.0 %fusion.9 = f32[2,128,704]{1,2,0:T(8,128)S(1)} fusion(f32[3,128,2048]{2,1,0:T(8,128)} %all-gather.20.cloned.1.call-done, f32[2,2048,704]{1,2,0:T(8,128)} %bitcast.65, f32[2,128,704]{1,2,0:T(8,128)S(1)} %multiply_add_fusion, f32[2]{0:T(128)S(1)} %bitcast.82), kind=kOutput, calls=%fused_computation.18 | convolution fusion | flops 4429725696 | bytes 16121864 | tf_op jit(solution)/shard_map/krs,ksc->krc/dot_general | solution.py:83
  327.9 102.1 %all-gather.22.cloned.1.call-done = f32[2048,1664]{0,1:T(8,128)} async-done(((f32[128,1664]{0,1:T(8,128)}), f32[2048,1664]{0,1:T(8,128)}) %all-gather.22.cloned.1.call-update) | async-done | bytes 13631504 | tf_op jit(solution)/shard_map/all_gather | solution.py:21
  429.9 10.4 %slice.61 = f32[2048,1408]{0,1:T(8,128)} slice(f32[2048,1664]{0,1:T(8,128)} %all-gather.22.cloned.1.call-done), slice={[0:2048], [0:1408]} | slice | bytes 23068672 | tf_op jit(solution)/shard_map/slice | solution.py:23
  440.3 9.2 fusion.26
  454.4 33.7 %reduce-scatter.6.cloned.1.call-done = f32[48,2048]{1,0:T(8,128)} async-done(((f32[384,2048]{1,0:T(8,128)}), f32[48,2048]{1,0:T(8,128)}) %reduce-scatter.6.cloned.1.call-update) | async-done | bytes 393232 | tf_op jit(solution)/shard_map/reduce_scatter | solution.py:38
  488.1 31.5 %all-gather.36.cloned.1.call-done = f32[384,2048]{1,0:T(8,128)} async-done(((f32[48,2048]{1,0:T(8,128)}), f32[384,2048]{1,0:T(8,128)}) %all-gather.36.cloned.1.call-update) | async-done | bytes 3145744 | tf_op jit(solution)/shard_map/all_gather | solution.py:41
  521.4 61.7 %all-gather.24.cloned.1.call-done = f32[3,2048,256]{2,1,0:T(8,128)} async-done(((f32[3,128,256]{2,1,0:T(8,128)}), f32[3,2048,256]{2,1,0:T(8,128)}) %all-gather.24.cloned.1.call-update) | async-done | bytes 6291472 | tf_op jit(solution)/shard_map/all_gather | solution.py:78
  591.8 27.5 %all-gather.26.cloned.1.call-done = f32[3,128,2048]{2,1,0:T(8,128)} async-done(((f32[3,128,256]{2,1,0:T(8,128)}), f32[3,128,2048]{2,1,0:T(8,128)}) %all-gather.26.cloned.1.call-update) | async-done | bytes 3145744 | tf_op jit(solution)/shard_map/all_gather | solution.py:81
  623.5 13.0 %convolution_add_fusion.1 = f32[2,128,704]{1,2,0:T(8,128)S(1)} fusion(f32[3,128,2048]{2,1,0:T(8,128)} %all-gather.26.cloned.1.call-done, f32[2,2048,704]{1,2,0:T(8,128)} %bitcast.69, f32[2,128,704]{1,2,0:T(8,128)S(1)} %fusion.9), kind=kOutput, calls=%fused_computation.16 | convolution fusion | flops 4429545472 | bytes 16121856 | tf_op jit(solution)/shard_map/krs,ksc->krc/dot_general | solution.py:83
  637.6 102.3 %all-gather.28.cloned.1.call-done = f32[2048,1664]{0,1:T(8,128)} async-done(((f32[128,1664]{0,1:T(8,128)}), f32[2048,1664]{0,1:T(8,128)}) %all-gather.28.cloned.1.call-update) | async-done | bytes 13631504 | tf_op jit(solution)/shard_map/all_gather | solution.py:21
  739.8 10.4 %slice.64 = f32[2048,1408]{0,1:T(8,128)} slice(f32[2048,1664]{0,1:T(8,128)} %all-gather.28.cloned.1.call-done), slice={[0:2048], [0:1408]} | slice | bytes 23068672 | tf_op jit(solution)/shard_map/slice | solution.py:23
  750.2 9.2 fusion.27
  764.2 33.7 %reduce-scatter.8.cloned.1.call-done = f32[48,2048]{1,0:T(8,128)} async-done(((f32[384,2048]{1,0:T(8,128)}), f32[48,2048]{1,0:T(8,128)}) %reduce-scatter.8.cloned.1.call-update) | async-done | bytes 393232 | tf_op jit(solution)/shard_map/reduce_scatter | solution.py:38
  798.0 31.5 %all-gather.38.cloned.1.call-done = f32[384,2048]{1,0:T(8,128)} async-done(((f32[48,2048]{1,0:T(8,128)}), f32[384,2048]{1,0:T(8,128)}) %all-gather.38.cloned.1.call-update) | async-done | bytes 3145744 | tf_op jit(solution)/shard_map/all_gather | solution.py:41
  831.5 61.4 %all-gather.30.cloned.1.call-done = f32[3,2048,256]{2,1,0:T(8,128)} async-done(((f32[3,128,256]{2,1,0:T(8,128)}), f32[3,2048,256]{2,1,0:T(8,128)}) %all-gather.30.cloned.1.call-update) | async-done | bytes 6291472 | tf_op jit(solution)/shard_map/all_gather | solution.py:78
  901.1 27.9 %all-gather.32.cloned.1.call-done = f32[3,128,2048]{2,1,0:T(8,128)} async-done(((f32[3,128,256]{2,1,0:T(8,128)}), f32[3,128,2048]{2,1,0:T(8,128)}) %all-gather.32.cloned.1.call-update) | async-done | bytes 3145744 | tf_op jit(solution)/shard_map/all_gather | solution.py:81
  934.0 13.9 %broadcast_multiply_fusion = (f32[2,128,704]{1,2,0:T(8,128)}, f32[2,128,704]{1,2,0:T(8,128)}) fusion(f32[2,128,704]{1,2,0:T(8,128)S(1)} %copy-done.3, f32[3,128,2048]{2,1,0:T(8,128)S(1)} %copy-done.1, f32[2,2048,704]{1,2,0:T(8,128)} %bitcast.67, f32[2,128,704]{1,2,0:T(8,128)S(1)} %convolution_add_fusion.1), kind=kOutput, calls=%fused_computation.38 | convolution fusion | flops 4430086144 | bytes 17563648 | tf_op jit(solution)/shard_map/krs,ksc->krc/dot_general | solution.py:83
  (70 shorter events, 66.3 us)
Async XLA Ops:
  7.2 109.6 %all-gather.16.cloned.1.call-start = ((), (), s32[]{:S(2)}) async-start(), calls=%async_computation.3 | async-start | bytes 14483456 | tf_op jit(solution)/shard_map/all_gather | solution.py:21
  8.2 300.5 %copy-start.2 = (f32[128,256]{1,0:T(8,128)}, f32[128,256]{1,0:T(8,128)S(1)}, u32[]{:S(2)}) copy-start(f32[128,256]{1,0:T(8,128)S(1)} %multiply_add_fusion.1) | copy-start | bytes 393220
  9.7 303.9 %copy-start = (f32[2,128,704]{1,2,0:T(8,128)}, f32[2,128,704]{1,2,0:T(8,128)S(1)}, u32[]{:S(2)}) copy-start(f32[2,128,704]{1,2,0:T(8,128)S(1)} %multiply_add_fusion) | copy-start | bytes 2162692
  10.8 164.1 %reduce-scatter.4.cloned.1.call-start = ((), (), s32[]{:S(2)}) async-start(), calls=%async_computation.4 | async-start | bytes 3538944 | tf_op jit(solution)/shard_map/reduce_scatter | solution.py:38
  141.2 65.3 %all-gather.34.cloned.1.call-start = ((), (), s32[]{:S(2)}) async-start(), calls=%async_computation.15 | async-start | bytes 3538944 | tf_op jit(solution)/shard_map/all_gather | solution.py:41
  174.9 100.9 %all-gather.18.cloned.1.call-start = ((), (), s32[]{:S(2)}) async-start(), calls=%async_computation.5 | async-start | bytes 6684672 | tf_op jit(solution)/shard_map/all_gather | solution.py:78
  208.2 100.5 %all-gather.20.cloned.1.call-start = ((), (), s32[]{:S(2)}) async-start(), calls=%async_computation.6 | async-start | bytes 3538944 | tf_op jit(solution)/shard_map/all_gather | solution.py:81
  284.1 145.9 %all-gather.22.cloned.1.call-start = ((), (), s32[]{:S(2)}) async-start(), calls=%async_computation.7 | async-start | bytes 14483456 | tf_op jit(solution)/shard_map/all_gather | solution.py:21
  327.6 160.4 %reduce-scatter.6.cloned.1.call-start = ((), (), s32[]{:S(2)}) async-start(), calls=%async_computation.8 | async-start | bytes 3538944 | tf_op jit(solution)/shard_map/reduce_scatter | solution.py:38
  454.3 65.3 %all-gather.36.cloned.1.call-start = ((), (), s32[]{:S(2)}) async-start(), calls=%async_computation.16 | async-start | bytes 3538944 | tf_op jit(solution)/shard_map/all_gather | solution.py:41
  488.1 95.1 %all-gather.24.cloned.1.call-start = ((), (), s32[]{:S(2)}) async-start(), calls=%async_computation.9 | async-start | bytes 6684672 | tf_op jit(solution)/shard_map/all_gather | solution.py:78
  521.4 97.9 %all-gather.26.cloned.1.call-start = ((), (), s32[]{:S(2)}) async-start(), calls=%async_computation.10 | async-start | bytes 3538944 | tf_op jit(solution)/shard_map/all_gather | solution.py:81
  591.3 148.5 %all-gather.28.cloned.1.call-start = ((), (), s32[]{:S(2)}) async-start(), calls=%async_computation.11 | async-start | bytes 14483456 | tf_op jit(solution)/shard_map/all_gather | solution.py:21
  637.5 160.4 %reduce-scatter.8.cloned.1.call-start = ((), (), s32[]{:S(2)}) async-start(), calls=%async_computation.12 | async-start | bytes 3538944 | tf_op jit(solution)/shard_map/reduce_scatter | solution.py:38
  764.2 65.3 %all-gather.38.cloned.1.call-start = ((), (), s32[]{:S(2)}) async-start(), calls=%async_computation.17 | async-start | bytes 3538944 | tf_op jit(solution)/shard_map/all_gather | solution.py:41
  797.9 94.9 %all-gather.30.cloned.1.call-start = ((), (), s32[]{:S(2)}) async-start(), calls=%async_computation.13 | async-start | bytes 6684672 | tf_op jit(solution)/shard_map/all_gather | solution.py:78
  831.2 97.8 %copy-start.4 = (f32[128,256]{1,0:T(8,128)S(1)}, f32[128,256]{1,0:T(8,128)}, u32[]{:S(2)}) copy-start(f32[128,256]{1,0:T(8,128)} %param.7) | copy-start | bytes 393220
  831.3 97.8 %all-gather.32.cloned.1.call-start = ((), (), s32[]{:S(2)}) async-start(), calls=%async_computation.14 | async-start | bytes 3538944 | tf_op jit(solution)/shard_map/all_gather | solution.py:81
  901.1 33.0 %copy-start.3 = (f32[2,128,704]{1,2,0:T(8,128)S(1)}, f32[2,128,704]{1,2,0:T(8,128)}, u32[]{:S(2)}) copy-start(f32[2,128,704]{1,2,0:T(8,128)} %param.6) | copy-start | bytes 2162692
  929.0 5.0 copy-start.1
Sparse Core Ops, SparseCore 0:
  10.9 105.7 all-gather.15
  141.3 33.5 reduce-scatter.3
  176.6 29.8 all-gather.33
  209.0 61.3 all-gather.17
  284.2 24.4 all-gather.19
  327.7 102.1 all-gather.21
  454.4 33.5 reduce-scatter.5
  489.7 29.8 all-gather.35
  522.3 60.7 all-gather.23
  591.5 27.7 all-gather.25
  637.6 102.1 all-gather.27
  764.3 33.5 reduce-scatter.7
  799.6 29.8 all-gather.37
  832.0 60.7 all-gather.29
  901.2 27.7 all-gather.31
where the time goes:
time: 963 us; the launch traced here: 955 us
  waiting for transfers between devices  708 us (74%)
  matrix products  114 us (12%)
  blocking collectives  67.5 us (7%)
  local copies, waits for them, and re-layouts  35.7 us (4%)
  between operations  14.3 us (1%)
  other arithmetic  13.1 us (1%)
    all_gather x3, waiting for transfers between devices, gather_turned(): lax.all_gather(both, axis, axis=0, tiled=True)  310 us
    all_gather x3, waiting for transfers between devices, local(): gram_cols = lax.all_gather(gram_block, 'fs', axis=1, tiled=True)  123 us
    reduce_scatter x3, waiting for transfers between devices, sum_by_parts(): lax.psum_scatter(rows_for(lines, lax.axis_size(axis)), axis, scatter_dime...  101 us
    all_gather x3, waiting for transfers between devices, sum_by_parts(): whole = lax.all_gather(own, axis).reshape(-1, *lines.shape[1:])  94.3 us
    all_gather x3, waiting for transfers between devices, local(): poly_rows = lax.all_gather(poly_mat, 'tp', axis=2, tiled=True)  79.3 us
    psum x1, blocking collectives, local(): scaling = scale_from(lax.psum(traces, ('fs', 'tp')))  67.5 us
    dot_general x3, matrix products, local(): jnp.einsum('krs,ksc->krc', poly_rows[:2], cols_in, precision=HIGH)  39.9 us
    slice x3, local copies, waits for them, and re-layouts, gather_turned(): share = result[:, at:at + t[0].size].reshape(-1, *t.shape[1:])  31.2 us
  transfers between devices with their start and end apart: 15, of which 14 were waited for; matrix products, arithmetic and copies ran while one was open for 0% of the time, Pallas kernels for 0%

commit v1 on v0

--- a/solution.py
+++ b/solution.py
@@ -75,7 +75,8 @@
             traces = block_trace(gram_block, fs_pos * row_count, tp_pos * block_width)
             scaling = scale_from(lax.psum(traces, ("fs", "tp")))
         factor = scaling if iteration == 0 else jnp.ones_like(scaling)
-        gram_cols = lax.all_gather(gram_block, "fs", axis=1, tiled=True)
+        sent = jnp.stack([gram_block] * lax.axis_size("fs"))
+        gram_cols = jnp.concatenate(lax.all_to_all(sent, "fs", 0, 0), axis=1)
         square = jnp.einsum("krs,ksc->krc", gram_rows, gram_cols, precision=HIGH)
         poly_mat = factor**2 * B_COEF * gram_block + factor**4 * C_COEF * square
         poly_rows = lax.all_gather(poly_mat, "tp", axis=2, tiled=True)

time: 963 us -> 1080 us (1.12)
  blocking collectives: 67.5 us -> 306 us
  waiting for transfers between devices: 708 us -> 571 us
  starting transfers between devices: 1.57 us -> 17.6 us
  matrix products: 114 us -> 103 us
    all_to_all x0 -> x2, blocking collectives: none -> 158 us  [local(): gram_cols = jnp.concatenate(lax.all_to_all(sent, 'fs', 0, 0), axis=1)]
    all_gather x3 -> x0, waiting for transfers between devices: 123 us -> none  [local(): gram_cols = lax.all_gather(gram_block, 'fs', axis=1, tiled=True)]
    psum x1, blocking collectives: 67.5 us -> 148 us  [local(): scaling = scale_from(lax.psum(traces, ('fs', 'tp')))]
    all_gather x3, waiting for transfers between devices: 79.3 us -> 65.4 us  [local(): poly_rows = lax.all_gather(poly_mat, 'tp', axis=2, tiled=True)]
    dot_general x3, matrix products: 24.6 us -> 13.7 us  [local(): square = jnp.einsum('krs,ksc->krc', gram_rows, gram_cols, precision=HIGH)]
  transfers between devices with their start and end apart: 15 -> 13, of which waited for: 14 -> 12; matrix products, arithmetic and copies ran while one was open for 0% -> 0% of each run, Pallas kernels for 0% -> 0%
where the time goes in v1:
time: 1080 us; the launch traced here: 1070 us
  waiting for transfers between devices  571 us (53%)
  blocking collectives  306 us (28%)
  matrix products  103 us (10%)
  local copies, waits for them, and re-layouts  46.5 us (4%)
  starting transfers between devices  17.6 us (2%)
  between operations  14.7 us (1%)
  other arithmetic  12.5 us (1%)
    all_gather x3, waiting for transfers between devices, gather_turned(): lax.all_gather(both, axis, axis=0, tiled=True)  310 us
    all_to_all x2, blocking collectives, local(): gram_cols = jnp.concatenate(lax.all_to_all(sent, 'fs', 0, 0), axis=1)  158 us
    psum x1, blocking collectives, local(): scaling = scale_from(lax.psum(traces, ('fs', 'tp')))  148 us
    reduce_scatter x3, waiting for transfers between devices, sum_by_parts(): lax.psum_scatter(rows_for(lines, lax.axis_size(axis)), axis, scatter_dime...  101 us
    all_gather x3, waiting for transfers between devices, sum_by_parts(): whole = lax.all_gather(own, axis).reshape(-1, *lines.shape[1:])  94.4 us
    all_gather x3, waiting for transfers between devices, local(): poly_rows = lax.all_gather(poly_mat, 'tp', axis=2, tiled=True)  65.4 us
    dot_general x3, matrix products, local(): jnp.einsum('krs,ksc->krc', poly_rows[:2], cols_in, precision=HIGH)  39.9 us
    slice x3, local copies, waits for them, and re-layouts, gather_turned(): share = result[:, at:at + t[0].size].reshape(-1, *t.shape[1:])  31.2 us
  transfers between devices with their start and end apart: 13, of which 12 were waited for; matrix products, arithmetic and copies ran while one was open for 0% of the time, Pallas kernels for 0%

profile of v1, /device:TPU:1, one launch (start us, length us, event | category | flops | bytes accessed | tf_op | source)
XLA Modules:
  0.0 1072.1 jit_solution(5101522628919980542)
XLA Ops:
  10.9 105.9 %all-gather.13.cloned.1.call-done = f32[2048,1664]{0,1:T(8,128)} async-done(((f32[128,1664]{0,1:T(8,128)}), f32[2048,1664]{0,1:T(8,128)}) %all-gather.13.cloned.1.call-update) | async-done | bytes 13631504 | tf_op jit(solution)/shard_map/all_gather | solution.py:21
  116.8 10.4 slice.58
  141.2 33.7 %reduce-scatter.4.cloned.1.call-done = f32[48,2048]{1,0:T(8,128)} async-done(((f32[384,2048]{1,0:T(8,128)}), f32[48,2048]{1,0:T(8,128)}) %reduce-scatter.4.cloned.1.call-update) | async-done | bytes 393232 | tf_op jit(solution)/shard_map/reduce_scatter | solution.py:38
  175.0 31.4 %all-gather.25.cloned.1.call-done = f32[384,2048]{1,0:T(8,128)} async-done(((f32[48,2048]{1,0:T(8,128)}), f32[384,2048]{1,0:T(8,128)}) %all-gather.25.cloned.1.call-update) | async-done | bytes 3145744 | tf_op jit(solution)/shard_map/all_gather | solution.py:41
  217.8 147.8 %psum.7 = f32[3]{0:T(128)S(1)} all-reduce(f32[3]{0:T(128)S(1)} %get-tuple-element.8), channel_id=1, replica_groups=mesh['fs'=16,'tp'=8] {'fs','tp'}, use_global_device_ids=true, to_apply=%region_2.3 | all-reduce | flops 3 | bytes 24 | tf_op jit(solution)/shard_map/psum | solution.py:76
  374.7 24.9 %all-gather.15.cloned.1.call-done = f32[3,128,2048]{2,1,0:T(8,128)} async-done(((f32[3,128,256]{2,1,0:T(8,128)}), f32[3,128,2048]{2,1,0:T(8,128)}) %all-gather.15.cloned.1.call-update) | async-done | bytes 3145744 | tf_op jit(solution)/shard_map/all_gather | solution.py:82
  404.5 13.0 %fusion.9 = f32[2,128,704]{1,2,0:T(8,128)S(1)} fusion(f32[3,128,2048]{2,1,0:T(8,128)} %all-gather.15.cloned.1.call-done, f32[2,2048,704]{1,2,0:T(8,128)} %bitcast.71, f32[2,128,704]{1,2,0:T(8,128)S(1)} %multiply_add_fusion, f32[2]{0:T(128)S(1)} %bitcast.93), kind=kOutput, calls=%fused_computation.18 | convolution fusion | flops 4429725696 | bytes 16121864 | tf_op jit(solution)/shard_map/krs,ksc->krc/dot_general | solution.py:84
  418.9 101.9 %all-gather.17.cloned.1.call-done = f32[2048,1664]{0,1:T(8,128)} async-done(((f32[128,1664]{0,1:T(8,128)}), f32[2048,1664]{0,1:T(8,128)}) %all-gather.17.cloned.1.call-update) | async-done | bytes 13631504 | tf_op jit(solution)/shard_map/all_gather | solution.py:21
  520.9 10.4 slice.61
  531.3 9.2 fusion.26
  545.3 33.6 %reduce-scatter.6.cloned.1.call-done = f32[48,2048]{1,0:T(8,128)} async-done(((f32[384,2048]{1,0:T(8,128)}), f32[48,2048]{1,0:T(8,128)}) %reduce-scatter.6.cloned.1.call-update) | async-done | bytes 393232 | tf_op jit(solution)/shard_map/reduce_scatter | solution.py:38
  579.0 31.5 %all-gather.27.cloned.1.call-done = f32[384,2048]{1,0:T(8,128)} async-done(((f32[48,2048]{1,0:T(8,128)}), f32[384,2048]{1,0:T(8,128)}) %all-gather.27.cloned.1.call-update) | async-done | bytes 3145744 | tf_op jit(solution)/shard_map/all_gather | solution.py:41
  612.3 79.1 %all_to_all.15 = f32[16,3,128,256]{3,2,1,0:T(8,128)S(1)} all-to-all(f32[16,3,128,256]{3,2,1,0:T(8,128)S(1)} %stack.7), channel_id=1, replica_groups=mesh['fs'=16,'tp'=8] {'fs'}, dimensions={0} | all-to-all | bytes 12582912 | tf_op jit(solution)/shard_map/all_to_all | solution.py:79
  697.9 9.9 all-gather.21.cloned.1.call-start
  707.8 15.3 %all-gather.19.cloned.1.call-done = f32[3,128,2048]{2,1,0:T(8,128)} async-done(((f32[3,128,256]{2,1,0:T(8,128)}), f32[3,128,2048]{2,1,0:T(8,128)}) %all-gather.19.cloned.1.call-update) | async-done | bytes 3145744 | tf_op jit(solution)/shard_map/all_gather | solution.py:82
  727.3 13.0 %convolution_add_fusion.1 = f32[2,128,704]{1,2,0:T(8,128)S(1)} fusion(f32[3,128,2048]{2,1,0:T(8,128)} %all-gather.19.cloned.1.call-done, f32[2,2048,704]{1,2,0:T(8,128)} %bitcast.75, f32[2,128,704]{1,2,0:T(8,128)S(1)} %fusion.9), kind=kOutput, calls=%fused_computation.16 | convolution fusion | flops 4429545472 | bytes 16121856 | tf_op jit(solution)/shard_map/krs,ksc->krc/dot_general | solution.py:84
  741.4 102.3 %all-gather.21.cloned.1.call-done = f32[2048,1664]{0,1:T(8,128)} async-done(((f32[128,1664]{0,1:T(8,128)}), f32[2048,1664]{0,1:T(8,128)}) %all-gather.21.cloned.1.call-update) | async-done | bytes 13631504 | tf_op jit(solution)/shard_map/all_gather | solution.py:21
  843.7 10.4 slice.64
  854.1 9.2 fusion.27
  868.1 33.7 %reduce-scatter.8.cloned.1.call-done = f32[48,2048]{1,0:T(8,128)} async-done(((f32[384,2048]{1,0:T(8,128)}), f32[48,2048]{1,0:T(8,128)}) %reduce-scatter.8.cloned.1.call-update) | async-done | bytes 393232 | tf_op jit(solution)/shard_map/reduce_scatter | solution.py:38
  901.8 31.5 %all-gather.29.cloned.1.call-done = f32[384,2048]{1,0:T(8,128)} async-done(((f32[48,2048]{1,0:T(8,128)}), f32[384,2048]{1,0:T(8,128)}) %all-gather.29.cloned.1.call-update) | async-done | bytes 3145744 | tf_op jit(solution)/shard_map/all_gather | solution.py:41
  935.1 79.3 %all_to_all.16 = f32[16,3,128,256]{3,2,1,0:T(8,128)S(1)} all-to-all(f32[16,3,128,256]{3,2,1,0:T(8,128)S(1)} %stack.8), channel_id=1, replica_groups=mesh['fs'=16,'tp'=8] {'fs'}, dimensions={0} | all-to-all | bytes 12582912 | tf_op jit(solution)/shard_map/all_to_all | solution.py:79
  1020.9 25.2 %all-gather.23.cloned.1.call-done = f32[3,128,2048]{2,1,0:T(8,128)} async-done(((f32[3,128,256]{2,1,0:T(8,128)}), f32[3,128,2048]{2,1,0:T(8,128)}) %all-gather.23.cloned.1.call-update) | async-done | bytes 3145744 | tf_op jit(solution)/shard_map/all_gather | solution.py:82
  1051.1 13.9 %broadcast_multiply_fusion = (f32[2,128,704]{1,2,0:T(8,128)}, f32[2,128,704]{1,2,0:T(8,128)}) fusion(f32[2,128,704]{1,2,0:T(8,128)S(1)} %copy-done.6, f32[3,128,2048]{2,1,0:T(8,128)S(1)} %copy-done.1, f32[2,2048,704]{1,2,0:T(8,128)} %bitcast.73, f32[2,128,704]{1,2,0:T(8,128)S(1)} %convolution_add_fusion.1), kind=kOutput, calls=%fused_computation.38 | convolution fusion | flops 4430086144 | bytes 17563648 | tf_op jit(solution)/shard_map/krs,ksc->krc/dot_general | solution.py:84
  (77 shorter events, 81.0 us)
Async XLA Ops:
  7.2 109.6 %all-gather.13.cloned.1.call-start = ((), (), s32[]{:S(2)}) async-start(), calls=%async_computation.6 | async-start | bytes 14483456 | tf_op jit(solution)/shard_map/all_gather | solution.py:21
  8.2 391.4 %copy-start.5 = (f32[128,256]{1,0:T(8,128)}, f32[128,256]{1,0:T(8,128)S(1)}, u32[]{:S(2)}) copy-start(f32[128,256]{1,0:T(8,128)S(1)} %multiply_add_fusion.1) | copy-start | bytes 393220
  9.7 394.8 %copy-start = (f32[2,128,704]{1,2,0:T(8,128)}, f32[2,128,704]{1,2,0:T(8,128)S(1)}, u32[]{:S(2)}) copy-start(f32[2,128,704]{1,2,0:T(8,128)S(1)} %multiply_add_fusion) | copy-start | bytes 2162692
  10.8 164.0 %reduce-scatter.4.cloned.1.call-start = ((), (), s32[]{:S(2)}) async-start(), calls=%async_computation.7 | async-start | bytes 3538944 | tf_op jit(solution)/shard_map/reduce_scatter | solution.py:38
  141.1 65.3 %all-gather.25.cloned.1.call-start = ((), (), s32[]{:S(2)}) async-start(), calls=%async_computation.15 | async-start | bytes 3538944 | tf_op jit(solution)/shard_map/all_gather | solution.py:41
  211.0 154.6 %all-to-all-start = ((f32[16,3,128,256]{3,2,1,0:T(8,128)}), f32[16,3,128,256]{3,2,1,0:T(8,128)}, u32[]{:S(2)}, u32[]{:S(2)}) async-start(f32[16,3,128,256]{3,2,1,0:T(8,128)} %stack.6), calls=%async_computation.1 | async-start | bytes 12582912 | tf_op jit(solution)/shard_map/all_to_all | solution.py:79
  217.8 181.9 %all-gather.15.cloned.1.call-start = ((), (), s32[]{:S(2)}) async-start(), calls=%async_computation.8 | async-start | bytes 3538944 | tf_op jit(solution)/shard_map/all_gather | solution.py:82
  365.6 3.7 copy-start.2
  373.9 147.0 %all-gather.17.cloned.1.call-start = ((), (), s32[]{:S(2)}) async-start(), calls=%async_computation.9 | async-start | bytes 14483456 | tf_op jit(solution)/shard_map/all_gather | solution.py:21
  418.6 160.4 %reduce-scatter.6.cloned.1.call-start = ((), (), s32[]{:S(2)}) async-start(), calls=%async_computation.10 | async-start | bytes 3538944 | tf_op jit(solution)/shard_map/reduce_scatter | solution.py:38
  545.2 65.2 %all-gather.27.cloned.1.call-start = ((), (), s32[]{:S(2)}) async-start(), calls=%async_computation.16 | async-start | bytes 3538944 | tf_op jit(solution)/shard_map/all_gather | solution.py:41
  579.0 144.1 %all-gather.19.cloned.1.call-start = ((), (), s32[]{:S(2)}) async-start(), calls=%async_computation.11 | async-start | bytes 3538944 | tf_op jit(solution)/shard_map/all_gather | solution.py:82
  691.4 1.9 copy-start.4
  697.9 145.8 %all-gather.21.cloned.1.call-start = ((), (), s32[]{:S(2)}) async-start(), calls=%async_computation.12 | async-start | bytes 14483456 | tf_op jit(solution)/shard_map/all_gather | solution.py:21
  741.3 160.4 %reduce-scatter.8.cloned.1.call-start = ((), (), s32[]{:S(2)}) async-start(), calls=%async_computation.13 | async-start | bytes 3538944 | tf_op jit(solution)/shard_map/reduce_scatter | solution.py:38
  868.0 65.3 %all-gather.29.cloned.1.call-start = ((), (), s32[]{:S(2)}) async-start(), calls=%async_computation.17 | async-start | bytes 3538944 | tf_op jit(solution)/shard_map/all_gather | solution.py:41
  901.8 144.3 %all-gather.23.cloned.1.call-start = ((), (), s32[]{:S(2)}) async-start(), calls=%async_computation.14 | async-start | bytes 3538944 | tf_op jit(solution)/shard_map/all_gather | solution.py:82
  1014.4 1.9 copy-start.3
  1016.3 29.8 %copy-start.7 = (f32[128,256]{1,0:T(8,128)S(1)}, f32[128,256]{1,0:T(8,128)}, u32[]{:S(2)}) copy-start(f32[128,256]{1,0:T(8,128)} %param.7) | copy-start | bytes 393220
  1020.9 30.2 %copy-start.6 = (f32[2,128,704]{1,2,0:T(8,128)S(1)}, f32[2,128,704]{1,2,0:T(8,128)}, u32[]{:S(2)}) copy-start(f32[2,128,704]{1,2,0:T(8,128)} %param.6) | copy-start | bytes 2162692
  1046.1 5.0 copy-start.1
Sparse Core Ops, SparseCore 0:
  10.9 105.7 all-gather.12
  141.3 33.5 reduce-scatter.3
  176.6 29.8 all-gather.24
  374.0 25.5 all-gather.14
  418.7 102.1 all-gather.16
  545.4 33.5 reduce-scatter.5
  580.6 29.8 all-gather.26
  698.0 25.0 all-gather.18
  741.5 102.1 all-gather.20
  868.1 33.5 reduce-scatter.7
  903.4 29.8 all-gather.28
  1021.0 25.0 all-gather.22
